TPU v7x, 128 devices: a whole 4x4x4 slice. The times are simulated.
128 devices in a mesh: sp: 16 (over z, y), fs: 4 (over x), tp: 2 (over core).
Axes of the slice: x: 4, y: 4, z: 4, core: 2. Of those that a mesh axis runs over, the one named last changes fastest.
Arguments:
- tokens: bfloat16 [8, 6144, 2048], P('fs', ('sp', 'tp')), may hold values from -6 to 6
- norm_gain: float32 [2048], replicated, may hold values from 0.1 to 1.9
- chain_entry: bfloat16 [2048, 2048], P(('sp', 'fs'), 'tp'), may hold values from -0.125 to 0.125
- pool_entry: bfloat16 [2048, 2048], P(('sp', 'fs'), 'tp'), may hold values from -0.125 to 0.125
- conv_taps: bfloat16 [4, 2048], P(None, 'tp'), may hold values from -3 to 3
- recur_gate: bfloat16 [8, 256, 256], P('tp'), may hold values from -0.375 to 0.375
- input_gate: bfloat16 [8, 256, 256], P('tp'), may hold values from -0.375 to 0.375
- decay_log: float32 [2048], P('tp'), may hold values from -9 to 5
- decay_shift: float32 [8, 6144, 2048], P('fs', 'sp', 'tp'), may hold values from -1 to 0
- start_state: float32 [8, 2048], P('fs', 'tp'), may hold values from -6 to 6
- pool_mix: bfloat16 [8, 256, 256], P('tp'), may hold values from -0.375 to 0.375
- pool_scale: float32 [2048], P('tp'), may hold values from 0.1 to 1.9
- chain_exit: bfloat16 [2048, 2048], P('tp', ('sp', 'fs')), may hold values from -0.09375 to 0.09375
- pool_exit: bfloat16 [2048, 2048], P('tp', ('sp', 'fs')), may hold values from -0.09375 to 0.09375
Outputs:
- mixed_rows: bfloat16 [8, 6144, 2048], P('fs', ('sp', 'tp'))
All inputs are finite; a program needn't handle non-finite values.
Results may differ from a plain program's by a relative error of at most 0.01.
Values may be sent and summed in bfloat16 or wider, within the bound.
A program may use at most 128 MiB of HBM per device.

v0:
```python
import jax
import jax.numpy as jnp
from jax import lax
from jax.experimental import pallas as pl
from jax.experimental.pallas import tpu as pltpu
from jax.sharding import PartitionSpec as P

MESH = pl.DeviceIdType.MESH
NORM_EPSILON = 1e-06
RECUR_SCALE = 8.0
HALO = 16
ROWS = 384
HALF = ROWS // 2
HEAD = 256
HEADS = 4
WIDTH = HEADS * HEAD
D = 2048
SEQ = 2
CHUNK = 128
STRIP = 32
ALL = slice(None)
F32 = jnp.float32
BF16 = jnp.bfloat16

ORDERS = ("xyz", "yzx", "zxy")
ARRAYS = (
    (0, ((0, 384), (384, 384), (768, 256))),
    (0, ((1024, 256), (1280, 384), (1664, 384))),
    (1, ((0, 384), (384, 256), (640, 384))),
    (1, ((1024, 384), (1408, 384), (1792, 256))),
)
MESSAGES = 24


def minus_expm1(v):
    series = v * (1.0 / 5040.0) + (1.0 / 720.0)
    for c in (1.0 / 120.0, 1.0 / 24.0, 1.0 / 6.0, 0.5, 1.0):
        series = series * v + c
    return jnp.where(v > -0.35, -v * series, 1.0 - jnp.exp(v))


def sigmoid(v):
    return 0.5 * jnp.tanh(0.5 * v) + 0.5


def kernel(
    tok_in, gain_ref, e_in, f_in, taps_ref, rgate_in, igate_in, dlog_ref, shift_in, start_ref,
    mix_in, scale_ref,
    out_ref,
    E, F, X, N, CP, A, B, G, rgate, igate, mix, R, CS, CR, OUTS, OUTR, OUTV,
    ssem, rsem, lsem, xsem, csend, crecv, osend, orecv, vsem,
):
    sp = lax.axis_index("sp")
    x = lax.axis_index("fs")
    c = lax.axis_index("tp")
    z = sp // 4
    y = sp % 4
    at = dict(x=x, y=y, z=z)
    after = lax.rem(sp + 1, 16)
    before = lax.rem(sp + 15, 16)

    place = {(d, by): lax.rem(at[d] + by + 4, 4) for d in "xyz" for by in (-1, 0, 1, 2)}

    def off(dim, by):
        return place[dim, by]

    def near(dim, by):
        p = dict(at)
        p[dim] = off(dim, by)
        return (p["z"] * 4 + p["y"], p["x"], c)

    own_rows = pl.ds(pl.multiple_of(HALO + c * HALF, 16), HALF)
    local = [
        pltpu.make_async_copy(src, dst, lsem.at[k])
        for k, (src, dst) in enumerate(
            (
                (e_in, E.at[z, y, x]),
                (tok_in, X.at[:, own_rows]),
                (f_in, F.at[z, y, x]),
                (shift_in, A),
                (rgate_in, rgate),
                (igate_in, igate),
                (mix_in, mix),
            )
        )
    ]
    for cp in local:
        cp.start()

    barrier = pltpu.get_barrier_semaphore()

    def greet(device):
        pl.semaphore_signal(barrier, inc=1, device_id=device, device_id_type=MESH)

    for by in (-1, 1):
        greet(near("x", by))
    greet((sp, x, 1 - c))
    for k in range(1, 16):
        greet((lax.rem(sp + k, 16), x, c))
    pl.semaphore_wait(barrier, 18)

    sent = []
    W = (E, F)

    def message(a, r, k, where, half, dim, by):
        buf, thirds = ARRAYS[a]
        lanes = pl.ds(*thirds[r])
        rows = (ALL, pl.ds(0, 16), pl.ds(16, 16))[half]
        v = W[buf].at[tuple(ALL if where[d] is None else where[d] for d in "zyx") + (rows, lanes)]
        return pltpu.make_async_remote_copy(
            src_ref=v, dst_ref=v, send_sem=ssem.at[a, r, k], recv_sem=rsem.at[a, r, k],
            device_id=near(dim, by), device_id_type=MESH,
        )

    def send(*args):
        cp = message(*args)
        cp.start()
        sent.append(args)

    def exchange(a, r, base, where, dim):
        for j, by in ((0, 1), (1, -1)):
            send(a, r, base + j, where, 0, dim, by)

    def shifted(where, dim, by):
        w = dict(where)
        w[dim] = off(dim, by)
        return w

    def pass_on(a, r, base, where, dim, side):
        w = shifted(where, dim, side)
        j = 0 if side == -1 else 1
        message(a, r, base + j, w, 0, dim, 1).wait_recv()
        send(a, r, base + 2 + j, w, 1 + j, dim, -side)

    def halves(a, r, base, where, dim):
        w = shifted(where, dim, 2)
        message(a, r, base + 2, w, 1, dim, 1).wait_recv()
        message(a, r, base + 3, w, 2, dim, 1).wait_recv()

    def w1(r):
        return dict(at)

    def w2(r):
        w = dict(at)
        w[ORDERS[r][0]] = None
        return w

    def w3(r, g):
        w = w2(r)
        w[ORDERS[r][1]] = off(ORDERS[r][1], (0, -1, 1, 2)[g])
        return w

    thirds = range(3)

    def s0(a):
        for r in thirds:
            exchange(a, r, 0, w1(r), ORDERS[r][0])

    def s1(a, side):
        for r in thirds:
            pass_on(a, r, 0, w1(r), ORDERS[r][0], side)

    def s2(a):
        for r in thirds:
            halves(a, r, 0, w1(r), ORDERS[r][0])
            exchange(a, r, 4, w2(r), ORDERS[r][1])
        for r in thirds:
            exchange(a, r, 8, w3(r, 0), ORDERS[r][2])

    def s3(a, side, g):
        for r in thirds:
            pass_on(a, r, 4, w2(r), ORDERS[r][1], side)
            exchange(a, r, 8 + 4 * g, w3(r, g), ORDERS[r][2])

    def s4(a, g, side):
        for r in thirds:
            pass_on(a, r, 8 + 4 * g, w3(r, g), ORDERS[r][2], side)

    def s5(a):
        for r in thirds:
            halves(a, r, 4, w2(r), ORDERS[r][1])
            exchange(a, r, 20, w3(r, 3), ORDERS[r][2])

    def s6(a):
        for g in range(4):
            for r in thirds:
                halves(a, r, 8 + 4 * g, w3(r, g), ORDERS[r][2])

    def stages(a):
        more = a + 1 < len(ARRAYS)
        steps = []
        if more:
            steps.append(lambda: s0(a + 1))
        steps.append(lambda: s3(a, -1, 1))
        steps.append(lambda: s3(a, 1, 2))
        if more:
            steps.append(lambda: s1(a + 1, -1))
            steps.append(lambda: s1(a + 1, 1))
        steps.append(lambda: s4(a, 0, -1))
        steps.append(lambda: s4(a, 0, 1))
        steps.append(lambda: s5(a))
        steps.append(lambda: s4(a, 1, -1))
        steps.append(lambda: s4(a, 1, 1))
        steps.append(lambda: s4(a, 2, -1))
        steps.append(lambda: s4(a, 2, 1))
        if more:
            steps.append(lambda: s2(a + 1))
        steps.append(lambda: s4(a, 3, -1))
        steps.append(lambda: s4(a, 3, 1))
        steps.append(lambda: s6(a))
        return steps

    def beside(steps, total, body):
        def one(i, carry):
            body(i)
            for k, step in enumerate(steps):
                pl.when(i == (k * total) // len(steps))(step)
            return carry
        lax.fori_loop(0, total, one, 0)

    local[0].wait()
    s0(0)
    local[1].wait()
    tok_copy = pltpu.make_async_remote_copy(
        src_ref=X.at[:, own_rows], dst_ref=X.at[:, own_rows], send_sem=xsem.at[0],
        recv_sem=xsem.at[1], device_id=(sp, x, 1 - c), device_id_type=MESH,
    )
    tok_copy.start()
    s1(0, -1)
    s1(0, 1)
    s2(0)
    other_rows = pl.ds(pl.multiple_of(HALO + (1 - c) * HALF, 16), HALF)
    pltpu.make_async_remote_copy(
        src_ref=X.at[:, other_rows], dst_ref=X.at[:, other_rows], send_sem=xsem.at[0],
        recv_sem=xsem.at[1], device_id=(sp, x, 1 - c), device_id_type=MESH,
    ).wait_recv()
    halo_copy = pltpu.make_async_remote_copy(
        src_ref=X.at[:, pl.ds(ROWS, HALO)], dst_ref=X.at[:, pl.ds(0, HALO)], send_sem=xsem.at[2],
        recv_sem=xsem.at[3], device_id=(after, x, c), device_id_type=MESH,
    )
    halo_copy.start()
    for k in range(2, 7):
        local[k].wait()

    first = jnp.where(sp == 0, 0.0, 1.0).astype(F32)

    def norm_tile(s, row, factor):
        v = X[s, pl.ds(row, 16), :].astype(F32)
        r = lax.rsqrt(jnp.mean(v * v, axis=-1, keepdims=True) + NORM_EPSILON)
        if factor is not None:
            r = r * factor
        N[s, pl.ds(row, 16), :] = (v * r * gain_ref[...]).astype(BF16)

    def norm_body(i):
        s = i // 24
        norm_tile(s, pl.multiple_of(HALO + (i % 24) * 16, 16), None)

    early = stages(0)
    early[0]()
    early[1]()
    early[2]()
    lax.fori_loop(0, 48, lambda i, q: (norm_body(i), q)[1], 0)
    for step in early[3:6]:
        step()
    halo_copy.wait_recv()
    for s in range(SEQ):
        norm_tile(s, 0, first)
    for step in early[6:]:
        step()

    def entry_tile(s, col):
        cols = pl.ds(col, HEAD)
        w = E[:, :, :, :, cols].reshape(D, HEAD)
        acc = jnp.dot(N[s], w, preferred_element_type=F32)
        CP[s, :, cols] = acc.astype(BF16).astype(F32)

    def entry_body(base):
        def body(i):
            entry_tile(i % 2, pl.multiple_of(base + (i // 2) * HEAD, HEAD))
        return body

    sub = lax.broadcasted_iota(jnp.int32, (STRIP, HEAD), 0) % 8

    def gates_body(i):
        h = i // 6
        s = (i // 3) % 2
        row = pl.multiple_of((i % 3) * CHUNK, CHUNK)
        cols = pl.ds(pl.multiple_of(h * HEAD, HEAD), HEAD)
        v = CP[s, pl.ds(row, CHUNK + HALO), cols]
        conv = pltpu.roll(v, 3, 0) * taps_ref[0:1, cols]
        conv = conv + pltpu.roll(v, 2, 0) * taps_ref[1:2, cols]
        conv = conv + pltpu.roll(v, 1, 0) * taps_ref[2:3, cols]
        conv = conv + v * taps_ref[3:4, cols]
        conv = conv[HALO:].astype(BF16)
        G[0] = jnp.dot(conv, rgate[h], preferred_element_type=F32)
        G[1] = jnp.dot(conv, igate[h], preferred_element_type=F32)
        G[2] = conv.astype(F32)
        rate = jnp.exp(dlog_ref[:, cols]) * (-RECUR_SCALE / 6144.0)
        for k in range(CHUNK // STRIP):
            rows = pl.ds(k * STRIP, STRIP)
            to = pl.ds(pl.multiple_of(row + k * STRIP, STRIP), STRIP)
            log_decay = sigmoid(G[0, rows]) * rate + A[s, to, cols]
            a = jnp.exp(log_decay)
            b = jnp.sqrt(minus_expm1(2.0 * log_decay)) * sigmoid(G[1, rows]) * G[2, rows]
            for d in (1, 2, 4):
                keep = sub >= d
                up_a = jnp.where(keep, pltpu.roll(a, d, 0), 1.0)
                up_b = jnp.where(keep, pltpu.roll(b, d, 0), 0.0)
                b = a * up_b + b
                a = a * up_a
            A[s, to, cols] = a
            B[s, to, cols] = b

    def scan_step(t, carry):
        out = []
        rows = pl.ds(pl.multiple_of(t * 8, 8), 8)
        for s in range(SEQ):
            ha, hb = carry[2 * s], carry[2 * s + 1]
            a, b = A[s, rows, :], B[s, rows, :]
            b = a * hb + b
            a = a * ha
            A[s, rows, :] = a
            B[s, rows, :] = b
            out.append(jnp.broadcast_to(a[7:8], (8, WIDTH)))
            out.append(jnp.broadcast_to(b[7:8], (8, WIDTH)))
        return tuple(out)

    def pool_group(g, i):
        w = 2 ** (g + 1)
        s = i // 3
        row = pl.multiple_of((i % 3) * CHUNK, CHUNK)
        cols = pl.ds(WIDTH + g * HEAD, HEAD)
        v = CP[s, pl.ds(row, CHUNK + HALO), cols]
        total = v
        for d in range(g + 1):
            total = total + pltpu.roll(total, 2 ** d, 0)
        position = (sp * ROWS + row + lax.broadcasted_iota(jnp.int32, (CHUNK, HEAD), 0)).astype(F32)
        share = 1.0 / jnp.minimum(position + 1.0, float(w))
        diff = (total[HALO:] * share - v[HALO:]).astype(BF16)
        mixed = jnp.dot(diff, mix[g], preferred_element_type=F32)
        R[s, pl.ds(row, CHUNK), cols] = (mixed * scale_ref[:, pl.ds(g * HEAD, HEAD)]).astype(BF16)

    def pool_body(i):
        for g in range(HEADS):
            pool_group(g, i)

    steps = stages(1)
    beside(steps[:6], 8, entry_body(0))
    beside(steps[6:], 24, gates_body)
    one = jnp.ones((8, WIDTH), F32)
    nought = jnp.zeros((8, WIDTH), F32)
    ends = lax.fori_loop(0, ROWS // 8, scan_step, (one, nought, one, nought))
    for s in range(SEQ):
        CS[pl.ds(s, 1), :] = ends[2 * s][0:1]
        CS[pl.ds(2 + s, 1), :] = ends[2 * s + 1][0:1]
    steps = stages(2)
    steps[0]()
    steps[1]()

    def carry_to(k):
        return pltpu.make_async_remote_copy(
            src_ref=CS, dst_ref=CR.at[sp], send_sem=csend.at[k], recv_sem=crecv.at[sp],
            device_id=(lax.rem(sp + k, 16), x, c), device_id_type=MESH,
        )

    def carry_from(j):
        return pltpu.make_async_remote_copy(
            src_ref=CS, dst_ref=CR.at[j], send_sem=csend.at[0], recv_sem=crecv.at[j],
            device_id=(j, x, c), device_id_type=MESH,
        )

    for k in range(1, 16):
        carry_to(k).start()
    beside(steps[2:9], 8, entry_body(WIDTH))
    beside(steps[9:14], 6, pool_body)
    for k in range(1, 16):
        carry_from(lax.rem(sp + 16 - k, 16)).wait_recv()
    h = start_ref[...]
    for j in range(15):
        h = jnp.where(j < sp, CR[j, 0:2, :] * h + CR[j, 2:4, :], h)

    def state_body(i):
        rows = pl.ds(pl.multiple_of(i * STRIP, STRIP), STRIP)
        for s in range(SEQ):
            R[s, rows, pl.ds(0, WIDTH)] = (A[s, rows, :] * h[s:s + 1] + B[s, rows, :]).astype(BF16)

    lax.fori_loop(0, ROWS // STRIP, lambda i, q: (state_body(i), q)[1], 0)
    for step in steps[14:]:
        step()

    mine = pl.ds(pl.multiple_of(c * HALF, 16), HALF)
    theirs = pl.ds(pl.multiple_of((1 - c) * HALF, 16), HALF)
    NT = (((1,), (1,)), ((), ()))

    def exit_weights(t, k0):
        return F[t // 2, pl.ds(2 * (t % 2), 2), :, :, pl.ds(k0, WIDTH)].reshape(HEAD, WIDTH)

    def chain_exit_body(t):
        cols = pl.ds(pl.multiple_of(t * HEAD, HEAD), HEAD)
        w = exit_weights(t, 0)
        for s in range(SEQ):
            CP[s, pl.ds(0, ROWS), cols] = lax.dot_general(
                R[s, :, pl.ds(0, WIDTH)], w, NT, preferred_element_type=F32
            )

    beside(stages(3), 8, chain_exit_body)

    def out_copy(t):
        cols = pl.ds(pl.multiple_of(t * HEAD, HEAD), HEAD)
        return pltpu.make_async_remote_copy(
            src_ref=OUTS.at[:, :, cols], dst_ref=OUTR.at[:, :, cols], send_sem=osend.at[t],
            recv_sem=orecv.at[t], device_id=(sp, x, 1 - c), device_id_type=MESH,
        )

    def write_out(t):
        cols = pl.ds(pl.multiple_of(t * HEAD, HEAD), HEAD)
        return pltpu.make_async_copy(OUTV.at[:, :, cols], out_ref.at[:, :, cols], vsem.at[t])

    def pool_exit_body(t):
        cols = pl.ds(pl.multiple_of(t * HEAD, HEAD), HEAD)
        w = exit_weights(t, WIDTH)
        for s in range(SEQ):
            OUTS[s, :, cols] = (
                lax.dot_general(
                    R[s, theirs, pl.ds(WIDTH, WIDTH)], w, NT, preferred_element_type=F32
                )
                + CP[s, theirs, cols]
            ).astype(BF16)
        for s in range(SEQ):
            CP[s, mine, cols] += lax.dot_general(
                R[s, mine, pl.ds(WIDTH, WIDTH)], w, NT, preferred_element_type=F32
            )
        out_copy(t).start()

    def finish(t):
        cols = pl.ds(pl.multiple_of(t * HEAD, HEAD), HEAD)
        out_copy(t).wait_recv()
        for s in range(SEQ):
            OUTV[s, :, cols] = (CP[s, mine, cols] + OUTR[s, :, cols].astype(F32)).astype(BF16)
        write_out(t).start()

    def last_body(t, q):
        pool_exit_body(t)

        @pl.when(t >= 3)
        def _():
            finish(t - 3)
        return q

    lax.fori_loop(0, 8, last_body, 0)
    for t in range(5, 8):
        finish(t)

    for args in sent:
        message(*args).wait_send()
    tok_copy.wait_send()
    halo_copy.wait_send()
    for k in range(1, 16):
        carry_to(k).wait_send()
    for t in range(8):
        out_copy(t).wait_send()
        write_out(t).wait()


def per_device(
    tokens, norm_gain, chain_entry, pool_entry, conv_taps, recur_gate, input_gate, decay_log,
    decay_shift, start_state, pool_mix, pool_scale, chain_exit, pool_exit,
):
    e = jnp.concatenate([chain_entry, pool_entry], axis=1)
    f = jnp.concatenate([chain_exit.T, pool_exit.T], axis=1)
    anywhere = pl.BlockSpec(memory_space=pl.ANY)
    vmem = pl.BlockSpec(memory_space=pltpu.VMEM)
    dma = pltpu.SemaphoreType.DMA
    return pl.pallas_call(
        kernel,
        out_shape=jax.ShapeDtypeStruct((SEQ, HALF, D), BF16),
        in_specs=[
            anywhere, vmem, anywhere, anywhere, vmem, anywhere, anywhere, vmem, anywhere, vmem,
            anywhere, vmem,
        ],
        out_specs=anywhere,
        scratch_shapes=[
            pltpu.VMEM((4, 4, 4, 32, D), BF16),
            pltpu.VMEM((4, 4, 4, 32, D), BF16),
            pltpu.VMEM((SEQ, HALO + ROWS, D), BF16),
            pltpu.VMEM((SEQ, HALO + ROWS, D), BF16),
            pltpu.VMEM((SEQ, HALO + ROWS, D), F32),
            pltpu.VMEM((SEQ, ROWS, WIDTH), F32),
            pltpu.VMEM((SEQ, ROWS, WIDTH), F32),
            pltpu.VMEM((3, CHUNK, HEAD), F32),
            pltpu.VMEM((HEADS, HEAD, HEAD), BF16),
            pltpu.VMEM((HEADS, HEAD, HEAD), BF16),
            pltpu.VMEM((HEADS, HEAD, HEAD), BF16),
            pltpu.VMEM((SEQ, ROWS, D), BF16),
            pltpu.VMEM((4, WIDTH), F32),
            pltpu.VMEM((16, 4, WIDTH), F32),
            pltpu.VMEM((SEQ, HALF, D), BF16),
            pltpu.VMEM((SEQ, HALF, D), BF16),
            pltpu.VMEM((SEQ, HALF, D), BF16),
            dma((len(ARRAYS), 3, MESSAGES)),
            dma((len(ARRAYS), 3, MESSAGES)),
            dma((7,)),
            dma((4,)),
            dma((16,)),
            dma((16,)),
            dma((8,)),
            dma((8,)),
            dma((8,)),
        ],
        compiler_params=pltpu.CompilerParams(
            collective_id=0, has_side_effects=True, vmem_limit_bytes=63 << 20
        ),
    )(
        tokens,
        norm_gain.reshape(1, D),
        e,
        f,
        conv_taps.astype(F32),
        recur_gate,
        input_gate,
        decay_log.reshape(1, WIDTH),
        decay_shift,
        start_state,
        pool_mix,
        pool_scale.reshape(1, WIDTH),
    )


def solution(mesh):
    in_specs = (
        P("fs", ("sp", "tp"), None),
        P(),
        P(("sp", "fs"), "tp"),
        P(("sp", "fs"), "tp"),
        P(None, "tp"),
        P("tp", None, None),
        P("tp", None, None),
        P("tp"),
        P("fs", "sp", "tp"),
        P("fs", "tp"),
        P("tp", None, None),
        P("tp"),
        P("tp", ("sp", "fs")),
        P("tp", ("sp", "fs")),
    )
    out_specs = P("fs", ("sp", "tp"), None)
    return jax.shard_map(
        per_device, mesh=mesh, in_specs=in_specs, out_specs=out_specs, check_vma=False
    )
```

profile of v0, /device:TPU:1, one launch (start us, length us, event | category | flops | bytes accessed | tf_op | source)
XLA Modules:
  0.0 121.8 jit_solution(7521259527139947721)
XLA Ops:
  0.0 1.3 %convert_element_type.3.taps_ref = f32[4,1024]{1,0:T(4,128)} convert(bf16[4,1024]{1,0:T(4,128)(2,1)} %param.18) | non-fusion elementwise | flops 4096 | bytes 24576 | tf_op jit(solution)/shard_map/convert_element_type | solution.py:518
  1.3 1.6 %pad_maximum_fusion = (bf16[32,2048]{1,0:T(8,128)(2,1)}, bf16[32,2048]{1,0:T(8,128)(2,1)}) fusion(bf16[32,1024]{1,0:T(8,128)(2,1)} %param.17, bf16[32,1024]{1,0:T(8,128)(2,1)} %param.16, bf16[32,1024]{1,0:T(8,128)(2,1)} %bitcast.5, bf16[32,1024]{1,0:T(8,128)(2,1)} %bitcast.6), kind=kLoop, calls=%fused_computation | loop fusion | flops 524288 | bytes 524288 | tf_op jit(solution)/shard_map/concatenate | solution.py:469
  2.9 116.1 %shard_map.136 = bf16[2,192,2048]{2,1,0:T(8,128)(2,1)} custom-call(bf16[2,192,2048]{2,1,0:T(8,128)(2,1)} %tok_in.1, f32[1,2048]{1,0:T(1,128)} %bitcast.7, bf16[32,2048]{1,0:T(8,128)(2,1)} %get-tuple-element.5.e_in, bf16[32,2048]{1,0:T(8,128)(2,1)} %get-tuple-element.6.f_in, f32[4,1024]{1,0:T(4,128)} %convert_element_type.3.taps_ref, ...), custom_call_target="tpu_custom_call" | custom-call | tf_op jit(solution)/shard_map/pallas_call | solution.py:474
  119.0 2.7 %copy.16 = bf16[2,192,2048]{2,1,0:T(8,128)(2,1)} copy(bf16[2,192,2048]{2,1,0:T(8,128)(2,1)} %shard_map.136) | data formatting | bytes 3145728
where the time goes:
time: 122 us
  Pallas kernels  116 us (95%)
  other arithmetic  2.94 us (2%)
  local copies, waits for them, and re-layouts  2.73 us (2%)
    pallas_call x1, Pallas kernels, per_device(): pl.pallas_call(kernel, out_shape=jax.ShapeDtypeStruct((SEQ, HALF, D), BF1...  116 us
    unnamed x1, local copies, waits for them, and re-layouts  2.73 us

commit v1 on v0

--- a/solution.py
+++ b/solution.py
@@ -1,3 +1,5 @@
+import heapq
+
 import jax
 import jax.numpy as jnp
 from jax import lax
@@ -32,6 +34,64 @@
 MESSAGES = 24
 
 
+RATE, HOP, LEAD, SLACK = 46.1e3, 2.3, 1.5, 0.3
+
+
+def needs(k):
+    j, g = k % 4, k // 4
+    if g == 0:
+        return () if j < 2 else (j - 2,)
+    if g == 1:
+        return (0, 1, 2, 3) if j < 2 else (j + 2,)
+    if j >= 2:
+        return (k - 2,)
+    return (0, 1, 2, 3) + ((), (4,), (5,), (6, 7))[g - 2]
+
+
+def rank(m):
+    a, r, k = m
+    g, late = k // 4, (k % 4) // 2
+    if g == 0:
+        return a * 10 - 35 + 0.1 * late
+    if g == 1:
+        return a * 10 - 12 + late
+    return a * 10 + (g - 2) + 1.5 * late
+
+
+def plan():
+    link, cost = {}, {}
+    for a, (_, split) in enumerate(ARRAYS):
+        for r in range(3):
+            for k in range(MESSAGES):
+                g = k // 4
+                link[a, r, k] = (ORDERS[r][min(g, 2)], k % 2)
+                size = (1 if g == 0 else 4) * 64 * split[r][1] / (1 + (k % 4) // 2)
+                cost[a, r, k] = size / RATE
+    order, arrives, free, times = [], {}, {}, [0.0]
+    left = sorted(link, key=rank)
+    while left:
+        now = heapq.heappop(times)
+        while times and times[0] <= now + 1e-5:
+            heapq.heappop(times)
+        here = {m for m, t in arrives.items() if t <= now + 1e-9}
+        rest = []
+        for m in left:
+            at = free.get(link[m], 0.0)
+            if not all((m[0], m[1], d) in here for d in needs(m[2])):
+                rest.append(m)
+            elif at - now > LEAD:
+                rest.append(m)
+                heapq.heappush(times, at - LEAD + 1e-5)
+            else:
+                free[link[m]] = max(now, at) + cost[m]
+                arrives[m] = free[link[m]] + HOP
+                order.append((now, m))
+                heapq.heappush(times, arrives[m])
+        left = rest
+    done = [max(t for m, t in arrives.items() if m[0] == a) for a in range(len(ARRAYS))]
+    return order, arrives, done
+
+
 def minus_expm1(v):
     series = v * (1.0 / 5040.0) + (1.0 / 720.0)
     for c in (1.0 / 120.0, 1.0 / 24.0, 1.0 / 6.0, 0.5, 1.0):
@@ -44,10 +104,10 @@
 
 
 def kernel(
-    tok_in, gain_ref, e_in, f_in, taps_ref, rgate_in, igate_in, dlog_ref, shift_in, start_ref,
+    tok_in, gain_ref, ec_in, ep_in, f_in, taps_ref, rgate_in, igate_in, dlog_ref, shift_in, start_ref,
     mix_in, scale_ref,
     out_ref,
-    E, F, X, N, CP, A, B, G, rgate, igate, mix, R, CS, CR, OUTS, OUTR, OUTV,
+    E, F, X, N, CP, A, B, G, rgate, igate, mix, R, CS, CR, CT, CZ, OUTS, OUTR, OUTV,
     ssem, rsem, lsem, xsem, csend, crecv, osend, orecv, vsem,
 ):
     sp = lax.axis_index("sp")
@@ -74,13 +134,14 @@
         pltpu.make_async_copy(src, dst, lsem.at[k])
         for k, (src, dst) in enumerate(
             (
-                (e_in, E.at[z, y, x]),
+                (ec_in, E.at[z, y, x, :, pl.ds(0, WIDTH)]),
                 (tok_in, X.at[:, own_rows]),
                 (f_in, F.at[z, y, x]),
                 (shift_in, A),
                 (rgate_in, rgate),
                 (igate_in, igate),
                 (mix_in, mix),
+                (ep_in, E.at[z, y, x, :, pl.ds(WIDTH, WIDTH)]),
             )
         )
     ]
@@ -95,9 +156,19 @@
     for by in (-1, 1):
         greet(near("x", by))
     greet((sp, x, 1 - c))
-    for k in range(1, 16):
-        greet((lax.rem(sp + k, 16), x, c))
-    pl.semaphore_wait(barrier, 18)
+    greet((after, x, c))
+    greet((before, x, c))
+
+    def along_y(k):
+        return (z * 4 + lax.rem(y + k, 4), x, c)
+
+    def along_z(k):
+        return (lax.rem(z + k, 4) * 4 + y, x, c)
+
+    for k in range(1, 4):
+        greet(along_y(k))
+        greet(along_z(k))
+    pl.semaphore_wait(barrier, 11)
 
     sent = []
     W = (E, F)
@@ -117,26 +188,11 @@
         cp.start()
         sent.append(args)
 
-    def exchange(a, r, base, where, dim):
-        for j, by in ((0, 1), (1, -1)):
-            send(a, r, base + j, where, 0, dim, by)
-
     def shifted(where, dim, by):
         w = dict(where)
         w[dim] = off(dim, by)
         return w
 
-    def pass_on(a, r, base, where, dim, side):
-        w = shifted(where, dim, side)
-        j = 0 if side == -1 else 1
-        message(a, r, base + j, w, 0, dim, 1).wait_recv()
-        send(a, r, base + 2 + j, w, 1 + j, dim, -side)
-
-    def halves(a, r, base, where, dim):
-        w = shifted(where, dim, 2)
-        message(a, r, base + 2, w, 1, dim, 1).wait_recv()
-        message(a, r, base + 3, w, 2, dim, 1).wait_recv()
-
     def w1(r):
         return dict(at)
 
@@ -150,85 +206,86 @@
         w[ORDERS[r][1]] = off(ORDERS[r][1], (0, -1, 1, 2)[g])
         return w
 
-    thirds = range(3)
-
-    def s0(a):
-        for r in thirds:
-            exchange(a, r, 0, w1(r), ORDERS[r][0])
-
-    def s1(a, side):
-        for r in thirds:
-            pass_on(a, r, 0, w1(r), ORDERS[r][0], side)
-
-    def s2(a):
-        for r in thirds:
-            halves(a, r, 0, w1(r), ORDERS[r][0])
-            exchange(a, r, 4, w2(r), ORDERS[r][1])
-        for r in thirds:
-            exchange(a, r, 8, w3(r, 0), ORDERS[r][2])
-
-    def s3(a, side, g):
-        for r in thirds:
-            pass_on(a, r, 4, w2(r), ORDERS[r][1], side)
-            exchange(a, r, 8 + 4 * g, w3(r, g), ORDERS[r][2])
-
-    def s4(a, g, side):
-        for r in thirds:
-            pass_on(a, r, 8 + 4 * g, w3(r, g), ORDERS[r][2], side)
-
-    def s5(a):
-        for r in thirds:
-            halves(a, r, 4, w2(r), ORDERS[r][1])
-            exchange(a, r, 20, w3(r, 3), ORDERS[r][2])
-
-    def s6(a):
-        for g in range(4):
-            for r in thirds:
-                halves(a, r, 8 + 4 * g, w3(r, g), ORDERS[r][2])
-
-    def stages(a):
-        more = a + 1 < len(ARRAYS)
-        steps = []
-        if more:
-            steps.append(lambda: s0(a + 1))
-        steps.append(lambda: s3(a, -1, 1))
-        steps.append(lambda: s3(a, 1, 2))
-        if more:
-            steps.append(lambda: s1(a + 1, -1))
-            steps.append(lambda: s1(a + 1, 1))
-        steps.append(lambda: s4(a, 0, -1))
-        steps.append(lambda: s4(a, 0, 1))
-        steps.append(lambda: s5(a))
-        steps.append(lambda: s4(a, 1, -1))
-        steps.append(lambda: s4(a, 1, 1))
-        steps.append(lambda: s4(a, 2, -1))
-        steps.append(lambda: s4(a, 2, 1))
-        if more:
-            steps.append(lambda: s2(a + 1))
-        steps.append(lambda: s4(a, 3, -1))
-        steps.append(lambda: s4(a, 3, 1))
-        steps.append(lambda: s6(a))
-        return steps
-
-    def beside(steps, total, body):
+    def where_of(r, k):
+        g = k // 4
+        return w1(r) if g == 0 else w2(r) if g == 1 else w3(r, g - 2)
+
+    def start(m):
+        a, r, k = m
+        dim = ORDERS[r][min(k // 4, 2)]
+        j = k % 4
+        where = where_of(r, k)
+        if j >= 2:
+            where = shifted(where, dim, -1 if j == 2 else 1)
+        send(a, r, k, where, 0 if j < 2 else j - 1, dim, 1 if j % 2 == 0 else -1)
+
+    def await_arrival(m):
+        a, r, k = m
+        dim = ORDERS[r][min(k // 4, 2)]
+        j = k % 4
+        by = (-1, 1, 2, 2)[j]
+        message(a, r, k, shifted(where_of(r, k), dim, by), 0 if j < 2 else j - 1, dim, 1).wait_recv()
+
+    order, arrives, done = plan()
+    waited = set()
+    todo = []
+    for t, m in order:
+        first_waits = [(m[0], m[1], d) for d in needs(m[2]) if (m[0], m[1], d) not in waited]
+        waited.update(first_waits)
+        todo.append((t + SLACK, first_waits, m))
+    clock = [0.0]
+
+    def perform(some):
+        for _, first_waits, m in some:
+            for w in first_waits:
+                await_arrival(w)
+            start(m)
+
+    def due(t):
+        n = 0
+        while n < len(todo) and todo[n][0] <= t:
+            n += 1
+        some = todo[:n]
+        del todo[:n]
+        return some
+
+    def until(t):
+        clock[0] = max(clock[0], t)
+        perform(due(clock[0]))
+
+    def gathered(a):
+        until(done[a])
+        for m in sorted((m for m in arrives if m[0] == a and m not in waited), key=arrives.get):
+            await_arrival(m)
+            waited.add(m)
+
+    def beside(total, each, body):
+        slots = []
+        for i in range(total):
+            some = due(clock[0] + i * each)
+            if some:
+                slots.append((i, some))
+        clock[0] += total * each
+
         def one(i, carry):
+            for k, some in slots:
+                pl.when(i == k)(lambda some=some: perform(some))
             body(i)
-            for k, step in enumerate(steps):
-                pl.when(i == (k * total) // len(steps))(step)
             return carry
+
         lax.fori_loop(0, total, one, 0)
 
     local[0].wait()
-    s0(0)
+    local[7].wait()
+    local[2].wait()
+    until(SLACK)
     local[1].wait()
     tok_copy = pltpu.make_async_remote_copy(
         src_ref=X.at[:, own_rows], dst_ref=X.at[:, own_rows], send_sem=xsem.at[0],
         recv_sem=xsem.at[1], device_id=(sp, x, 1 - c), device_id_type=MESH,
     )
     tok_copy.start()
-    s1(0, -1)
-    s1(0, 1)
-    s2(0)
+    until(5.0)
     other_rows = pl.ds(pl.multiple_of(HALO + (1 - c) * HALF, 16), HALF)
     pltpu.make_async_remote_copy(
         src_ref=X.at[:, other_rows], dst_ref=X.at[:, other_rows], send_sem=xsem.at[0],
@@ -239,7 +296,7 @@
         recv_sem=xsem.at[3], device_id=(after, x, c), device_id_type=MESH,
     )
     halo_copy.start()
-    for k in range(2, 7):
+    for k in range(3, 7):
         local[k].wait()
 
     first = jnp.where(sp == 0, 0.0, 1.0).astype(F32)
@@ -255,18 +312,11 @@
         s = i // 24
         norm_tile(s, pl.multiple_of(HALO + (i % 24) * 16, 16), None)
 
-    early = stages(0)
-    early[0]()
-    early[1]()
-    early[2]()
-    lax.fori_loop(0, 48, lambda i, q: (norm_body(i), q)[1], 0)
-    for step in early[3:6]:
-        step()
+    beside(48, 0.07, norm_body)
+    until(11.0)
     halo_copy.wait_recv()
     for s in range(SEQ):
         norm_tile(s, 0, first)
-    for step in early[6:]:
-        step()
 
     def entry_tile(s, col):
         cols = pl.ds(col, HEAD)
@@ -287,10 +337,11 @@
         row = pl.multiple_of((i % 3) * CHUNK, CHUNK)
         cols = pl.ds(pl.multiple_of(h * HEAD, HEAD), HEAD)
         v = CP[s, pl.ds(row, CHUNK + HALO), cols]
-        conv = pltpu.roll(v, 3, 0) * taps_ref[0:1, cols]
-        conv = conv + pltpu.roll(v, 2, 0) * taps_ref[1:2, cols]
-        conv = conv + pltpu.roll(v, 1, 0) * taps_ref[2:3, cols]
-        conv = conv + v * taps_ref[3:4, cols]
+        taps = taps_ref[:, cols].astype(F32)
+        conv = pltpu.roll(v, 3, 0) * taps[0:1]
+        conv = conv + pltpu.roll(v, 2, 0) * taps[1:2]
+        conv = conv + pltpu.roll(v, 1, 0) * taps[2:3]
+        conv = conv + v * taps[3:4]
         conv = conv[HALO:].astype(BF16)
         G[0] = jnp.dot(conv, rgate[h], preferred_element_type=F32)
         G[1] = jnp.dot(conv, igate[h], preferred_element_type=F32)
@@ -344,49 +395,62 @@
         for g in range(HEADS):
             pool_group(g, i)
 
-    steps = stages(1)
-    beside(steps[:6], 8, entry_body(0))
-    beside(steps[6:], 24, gates_body)
+    gathered(0)
+    beside(8, 0.5, entry_body(0))
+    beside(24, 0.53, gates_body)
     one = jnp.ones((8, WIDTH), F32)
     nought = jnp.zeros((8, WIDTH), F32)
     ends = lax.fori_loop(0, ROWS // 8, scan_step, (one, nought, one, nought))
+    until(clock[0] + 1.0)
     for s in range(SEQ):
         CS[pl.ds(s, 1), :] = ends[2 * s][0:1]
         CS[pl.ds(2 + s, 1), :] = ends[2 * s + 1][0:1]
-    steps = stages(2)
-    steps[0]()
-    steps[1]()
-
-    def carry_to(k):
+
+    def carry(src, held, mine, k, device):
+        base = 0 if held is CR else 4
         return pltpu.make_async_remote_copy(
-            src_ref=CS, dst_ref=CR.at[sp], send_sem=csend.at[k], recv_sem=crecv.at[sp],
-            device_id=(lax.rem(sp + k, 16), x, c), device_id_type=MESH,
+            src_ref=src, dst_ref=held.at[mine], send_sem=csend.at[base + k],
+            recv_sem=crecv.at[base + mine], device_id=device, device_id_type=MESH,
         )
 
-    def carry_from(j):
-        return pltpu.make_async_remote_copy(
-            src_ref=CS, dst_ref=CR.at[j], send_sem=csend.at[0], recv_sem=crecv.at[j],
-            device_id=(j, x, c), device_id_type=MESH,
-        )
-
-    for k in range(1, 16):
-        carry_to(k).start()
-    beside(steps[2:9], 8, entry_body(WIDTH))
-    beside(steps[9:14], 6, pool_body)
-    for k in range(1, 16):
-        carry_from(lax.rem(sp + 16 - k, 16)).wait_recv()
+    def to_y(k):
+        return carry(CS, CR, y, k, along_y(k))
+
+    def to_z(k):
+        return carry(CT, CZ, z, k, along_z(k))
+
+    CR[y] = CS[...]
+    for k in range(1, 4):
+        to_y(k).start()
+    gathered(1)
+    beside(8, 0.5, entry_body(WIDTH))
+    for k in range(1, 4):
+        carry(CS, CR, lax.rem(y + 4 - k, 4), k, along_y(k)).wait_recv()
+    row_a, row_b = CR[0, 0:2, :], CR[0, 2:4, :]
+    for j in range(1, 4):
+        row_b = CR[j, 0:2, :] * row_b + CR[j, 2:4, :]
+        row_a = CR[j, 0:2, :] * row_a
+    CT[pl.ds(0, 2), :] = row_a
+    CT[pl.ds(2, 2), :] = row_b
+    beside(3, 0.4, pool_body)
+    for k in range(1, 4):
+        to_z(k).start()
+    beside(3, 0.4, lambda i: pool_body(i + 3))
+    for k in range(1, 4):
+        carry(CT, CZ, lax.rem(z + 4 - k, 4), k, along_z(k)).wait_recv()
     h = start_ref[...]
-    for j in range(15):
-        h = jnp.where(j < sp, CR[j, 0:2, :] * h + CR[j, 2:4, :], h)
+    for j in range(3):
+        h = jnp.where(j < z, CZ[j, 0:2, :] * h + CZ[j, 2:4, :], h)
+    for j in range(3):
+        h = jnp.where(j < y, CR[j, 0:2, :] * h + CR[j, 2:4, :], h)
 
     def state_body(i):
         rows = pl.ds(pl.multiple_of(i * STRIP, STRIP), STRIP)
         for s in range(SEQ):
             R[s, rows, pl.ds(0, WIDTH)] = (A[s, rows, :] * h[s:s + 1] + B[s, rows, :]).astype(BF16)
 
-    lax.fori_loop(0, ROWS // STRIP, lambda i, q: (state_body(i), q)[1], 0)
-    for step in steps[14:]:
-        step()
+    beside(ROWS // STRIP, 0.05, state_body)
+    gathered(2)
 
     mine = pl.ds(pl.multiple_of(c * HALF, 16), HALF)
     theirs = pl.ds(pl.multiple_of((1 - c) * HALF, 16), HALF)
@@ -403,7 +467,8 @@
                 R[s, :, pl.ds(0, WIDTH)], w, NT, preferred_element_type=F32
             )
 
-    beside(stages(3), 8, chain_exit_body)
+    beside(8, 0.57, chain_exit_body)
+    gathered(3)
 
     def out_copy(t):
         cols = pl.ds(pl.multiple_of(t * HEAD, HEAD), HEAD)
@@ -455,8 +520,9 @@
         message(*args).wait_send()
     tok_copy.wait_send()
     halo_copy.wait_send()
-    for k in range(1, 16):
-        carry_to(k).wait_send()
+    for k in range(1, 4):
+        to_y(k).wait_send()
+        to_z(k).wait_send()
     for t in range(8):
         out_copy(t).wait_send()
         write_out(t).wait()
@@ -466,7 +532,6 @@
     tokens, norm_gain, chain_entry, pool_entry, conv_taps, recur_gate, input_gate, decay_log,
     decay_shift, start_state, pool_mix, pool_scale, chain_exit, pool_exit,
 ):
-    e = jnp.concatenate([chain_entry, pool_entry], axis=1)
     f = jnp.concatenate([chain_exit.T, pool_exit.T], axis=1)
     anywhere = pl.BlockSpec(memory_space=pl.ANY)
     vmem = pl.BlockSpec(memory_space=pltpu.VMEM)
@@ -475,7 +540,7 @@
         kernel,
         out_shape=jax.ShapeDtypeStruct((SEQ, HALF, D), BF16),
         in_specs=[
-            anywhere, vmem, anywhere, anywhere, vmem, anywhere, anywhere, vmem, anywhere, vmem,
+            anywhere, vmem, anywhere, anywhere, anywhere, vmem, anywhere, anywhere, vmem, anywhere, vmem,
             anywhere, vmem,
         ],
         out_specs=anywhere,
@@ -493,16 +558,18 @@
             pltpu.VMEM((HEADS, HEAD, HEAD), BF16),
             pltpu.VMEM((SEQ, ROWS, D), BF16),
             pltpu.VMEM((4, WIDTH), F32),
-            pltpu.VMEM((16, 4, WIDTH), F32),
+            pltpu.VMEM((4, 4, WIDTH), F32),
+            pltpu.VMEM((4, WIDTH), F32),
+            pltpu.VMEM((4, 4, WIDTH), F32),
             pltpu.VMEM((SEQ, HALF, D), BF16),
             pltpu.VMEM((SEQ, HALF, D), BF16),
             pltpu.VMEM((SEQ, HALF, D), BF16),
             dma((len(ARRAYS), 3, MESSAGES)),
             dma((len(ARRAYS), 3, MESSAGES)),
-            dma((7,)),
+            dma((8,)),
             dma((4,)),
-            dma((16,)),
-            dma((16,)),
+            dma((8,)),
+            dma((8,)),
             dma((8,)),
             dma((8,)),
             dma((8,)),
@@ -513,9 +580,10 @@
     )(
         tokens,
         norm_gain.reshape(1, D),
-        e,
+        chain_entry,
+        pool_entry,
         f,
-        conv_taps.astype(F32),
+        conv_taps,
         recur_gate,
         input_gate,
         decay_log.reshape(1, WIDTH),

time: 122 us -> 110 us (0.902)
  Pallas kernels: 116 us -> 106 us
  other arithmetic: 2.94 us -> 1.53 us
    pallas_call x1, Pallas kernels: 116 us -> 106 us  [per_device(): pl.pallas_call(kernel, out_shape=jax.ShapeDtypeStruct((SEQ, HALF, D), BF1...]
    convert_element_type x1 -> x0, other arithmetic: 1.3 us -> none  [per_device(): conv_taps.astype(F32)]
where the time goes in v1:
time: 110 us
  Pallas kernels  106 us (96%)
  local copies, waits for them, and re-layouts  2.73 us (2%)
  other arithmetic  1.53 us (1%)
    pallas_call x1, Pallas kernels, per_device(): pl.pallas_call(kernel, out_shape=jax.ShapeDtypeStruct((SEQ, HALF, D), BF1...  106 us
    unnamed x1, local copies, waits for them, and re-layouts  2.73 us

profile of v1, /device:TPU:1, one launch (start us, length us, event | category | flops | bytes accessed | tf_op | source)
XLA Modules:
  0.0 110.1 jit_solution(16585418966521894128)
XLA Ops:
  0.0 1.5 %pad_maximum_fusion.f_in = bf16[32,2048]{1,0:T(8,128)(2,1)} fusion(bf16[32,1024]{1,0:T(8,128)(2,1)} %bitcast.5, bf16[32,1024]{1,0:T(8,128)(2,1)} %bitcast.6), kind=kLoop, calls=%fused_computation | loop fusion | flops 262144 | bytes 262144 | tf_op jit(solution)/shard_map/concatenate | solution.py:535
  1.5 105.8 %shard_map.136 = bf16[2,192,2048]{2,1,0:T(8,128)(2,1)} custom-call(bf16[2,192,2048]{2,1,0:T(8,128)(2,1)} %tok_in.1, f32[1,2048]{1,0:T(1,128)} %bitcast.7, bf16[32,1024]{1,0:T(8,128)(2,1)} %ec_in.1, bf16[32,1024]{1,0:T(8,128)(2,1)} %ep_in.1, bf16[32,2048]{1,0:T(8,128)(2,1)} %pad_maximum_fusion.f_in, bf16[4,1024]{1,0:T(4,128)(2,1)} %taps_ref.1, ...), custom_call_target="tpu_custom_call" | custom-call | tf_op jit(solution)/shard_map/pallas_call | solution.py:539
  107.3 2.7 %copy.16 = bf16[2,192,2048]{2,1,0:T(8,128)(2,1)} copy(bf16[2,192,2048]{2,1,0:T(8,128)(2,1)} %shard_map.136) | data formatting | bytes 3145728

commit v2 on v1

--- a/solution.py
+++ b/solution.py
@@ -19,7 +19,7 @@
 D = 2048
 SEQ = 2
 CHUNK = 128
-STRIP = 32
+STRIP = 16
 ALL = slice(None)
 F32 = jnp.float32
 BF16 = jnp.bfloat16
@@ -34,7 +34,7 @@
 MESSAGES = 24
 
 
-RATE, HOP, LEAD, SLACK = 46.1e3, 2.3, 1.5, 0.3
+RATE, HOP, LEAD, SLACK = 55e3, 1.8, 1.5, 0.0
 
 
 def needs(k):
@@ -253,8 +253,18 @@
         clock[0] = max(clock[0], t)
         perform(due(clock[0]))
 
+    when = {m: t for t, m in order}
+    settled = set()
+
+    def settle(t):
+        for args in sent:
+            if args[:3] not in settled and when[args[:3]] <= t:
+                message(*args).wait_send()
+                settled.add(args[:3])
+
     def gathered(a):
         until(done[a])
+        settle(done[a] - 8.0)
         for m in sorted((m for m in arrives if m[0] == a and m not in waited), key=arrives.get):
             await_arrival(m)
             waited.add(m)
@@ -516,8 +526,7 @@
     for t in range(5, 8):
         finish(t)
 
-    for args in sent:
-        message(*args).wait_send()
+    settle(1e9)
     tok_copy.wait_send()
     halo_copy.wait_send()
     for k in range(1, 4):

time: 110 us -> 108 us (0.982)
  Pallas kernels: 106 us -> 104 us
    pallas_call x1, Pallas kernels: 106 us -> 104 us  [per_device(): pl.pallas_call(kernel, out_shape=jax.ShapeDtypeStruct((SEQ, HALF, D), BF1...]
where the time goes in v2:
time: 108 us
  Pallas kernels  104 us (96%)
  local copies, waits for them, and re-layouts  2.73 us (3%)
  other arithmetic  1.53 us (1%)
    pallas_call x1, Pallas kernels, per_device(): pl.pallas_call(kernel, out_shape=jax.ShapeDtypeStruct((SEQ, HALF, D), BF1...  104 us
    unnamed x1, local copies, waits for them, and re-layouts  2.73 us

profile of v2, /device:TPU:1, one launch (start us, length us, event | category | flops | bytes accessed | tf_op | source)
XLA Modules:
  0.0 108.1 jit_solution(16123425816510697044)
XLA Ops:
  0.0 1.5 %pad_maximum_fusion.f_in = bf16[32,2048]{1,0:T(8,128)(2,1)} fusion(bf16[32,1024]{1,0:T(8,128)(2,1)} %bitcast.5, bf16[32,1024]{1,0:T(8,128)(2,1)} %bitcast.6), kind=kLoop, calls=%fused_computation | loop fusion | flops 262144 | bytes 262144 | tf_op jit(solution)/shard_map/concatenate | solution.py:544
  1.5 103.9 %shard_map.136 = bf16[2,192,2048]{2,1,0:T(8,128)(2,1)} custom-call(bf16[2,192,2048]{2,1,0:T(8,128)(2,1)} %tok_in.1, f32[1,2048]{1,0:T(1,128)} %bitcast.7, bf16[32,1024]{1,0:T(8,128)(2,1)} %ec_in.1, bf16[32,1024]{1,0:T(8,128)(2,1)} %ep_in.1, bf16[32,2048]{1,0:T(8,128)(2,1)} %pad_maximum_fusion.f_in, bf16[4,1024]{1,0:T(4,128)(2,1)} %taps_ref.1, ...), custom_call_target="tpu_custom_call" | custom-call | tf_op jit(solution)/shard_map/pallas_call | solution.py:548
  105.4 2.7 %copy.16 = bf16[2,192,2048]{2,1,0:T(8,128)(2,1)} copy(bf16[2,192,2048]{2,1,0:T(8,128)(2,1)} %shard_map.136) | data formatting | bytes 3145728
